TPU v7x, 512 devices: a whole 4x8x8 slice. The times are simulated.
512 devices in a mesh: ep: 32 (over z, x), tp: 16 (over y, core).
Axes of the slice: x: 4, y: 8, z: 8, core: 2. Of those that a mesh axis runs over, the one named last changes fastest.
Arguments:
- queries: bfloat16 [8192, 2048], P('ep', 'tp'), may hold values from -9 to 9
- key_rows: bfloat16 [8192, 2048], P('ep', 'tp'), may hold values from -9 to 9
- values: bfloat16 [8192, 2048], P('ep', 'tp'), may hold values from -6 to 6
- second_scale: float32 [16], P('tp'), may hold values from 0.3 to 0.8
- head_gain: float32 [128], replicated, may hold values from 0.1 to 1.9
- out_weight: bfloat16 [2048, 2048], P(None, 'tp'), may hold values from -0.125 to 0.125
- routed_in: bfloat16 [8192, 2048], P('ep'), may hold values from -6 to 6
- routed_gain: float32 [2048], replicated, may hold values from 0.1 to 1.9
- expert_ids: int32 [8192, 2], P('ep'), may hold values from 0 to 31, all different within a row; in each aligned block of 256 rows (0 to 255, 256 to 511, ...) at most 32 rows name the same one
- group_logits: float32 [8192, 8], P('ep'), may hold values from -6 to 6
- inner_logits: float32 [8192, 2], P('ep'), may hold values from -6 to 6
- gate_weight: bfloat16 [32, 2048, 4096], P('ep', None, 'tp'), may hold values from -0.125 to 0.125
- up_weight: bfloat16 [32, 2048, 4096], P('ep', None, 'tp'), may hold values from -0.125 to 0.125
- down_weight: bfloat16 [32, 4096, 2048], P('ep', 'tp'), may hold values from -0.09375 to 0.09375
Outputs:
- mixer_out: bfloat16 [8192, 2048], P('ep', 'tp')
- routed_out: bfloat16 [8192, 2048], P('ep', 'tp')
Inputs may be any that keep to these rules, and one draw needn't show every extreme that they name: `expert_ids`: the two ids of a row differ. In the rows of one device (aligned blocks of 256 rows) no expert is named by more than 32 rows, a bound that some block reaches.
All inputs are finite; a program needn't handle non-finite values.
Results may differ from a plain program's by a relative error of at most 0.018.
Values may be sent and summed in bfloat16 or wider, within the bound.
A program may use at most 128 MiB of HBM per device.

v0:
```python
import math
import jax
import jax.numpy as jnp
from jax import lax
from jax.sharding import Mesh
from jax.sharding import PartitionSpec as P

GROUP_SIZE = 4
EP = ("ep_0", "ep_1")
EPSILON = 1e-05
LOWEST = -1e30


def whole_of(array, axes, dim):
    if not axes:
        return array
    nearer = lax.all_gather(array, axes[-1], axis=dim, tiled=True)
    return whole_of(nearer, axes[:-1], dim)


def token_mixer(queries, key_rows, values, second_scale, head_gain, out_weight):
    row_count = queries.shape[0]
    local_heads = second_scale.shape[0]
    qk_size = queries.shape[1] // (2 * local_heads)
    value_size = values.shape[1] // local_heads
    first_pos = lax.axis_index(EP) * row_count
    query_pos = first_pos + jnp.arange(row_count, dtype=jnp.int32)
    last_pos = first_pos + row_count - 1
    query_four = queries.reshape(row_count, local_heads, 2, qk_size)
    score_scale = qk_size ** (-0.5)
    initial = (
        jnp.full((row_count, local_heads, 2), LOWEST, jnp.float32),
        jnp.zeros((row_count, local_heads, 2), jnp.float32),
        jnp.zeros((row_count, local_heads, 2, value_size), jnp.float32),
    )
    state_now = initial
    key_piece = whole_of(key_rows, EP, 0)
    value_piece = whole_of(values, EP, 0)
    piece_count = key_piece.shape[0]
    block_width = math.gcd(piece_count, 512)
    blocks = piece_count // block_width
    key_blocks = key_piece.reshape(blocks, block_width, local_heads, 2, qk_size)
    value_blocks = value_piece.reshape(blocks, block_width, local_heads, value_size)

    def update(state_inner, block_index):
        key_start = block_index * block_width

        def attend(inner_state):
            running_max, denominator, weighted = inner_state
            scores = (
                jnp.einsum(
                    "qhmd,khmd->qhmk",
                    query_four,
                    key_blocks[block_index],
                    preferred_element_type=jnp.float32,
                )
                * score_scale
            )
            key_pos = key_start + jnp.arange(block_width, dtype=jnp.int32)
            visible = (query_pos[:, None] >= key_pos[None, :])[:, None, None, :]
            scores = jnp.where(visible, scores, LOWEST)
            new_max = jnp.maximum(running_max, jnp.max(scores, axis=-1))
            exp_terms = jnp.where(visible, jnp.exp(scores - new_max[..., None]), 0.0)
            factor = jnp.exp(running_max - new_max)
            denominator = denominator * factor + jnp.sum(exp_terms, axis=-1)
            weighted = weighted * factor[..., None] + jnp.einsum(
                "qhmk,khe->qhme",
                exp_terms.astype(jnp.bfloat16),
                value_blocks[block_index],
                preferred_element_type=jnp.float32,
            )
            return (new_max, denominator, weighted)

        return (
            lax.cond(key_start <= last_pos, attend, lambda inner_state: inner_state, state_inner),
            None,
        )

    state_now, _ = lax.scan(update, state_now, jnp.arange(blocks, dtype=jnp.int32))
    running_max, denominator, weighted = state_now
    mapped = weighted / denominator[..., None]
    difference = mapped[:, :, 0] - second_scale[None, :, None] * mapped[:, :, 1]
    inv_norm = lax.rsqrt(jnp.mean(difference * difference, axis=-1, keepdims=True) + EPSILON)
    head_out = (
        (difference * inv_norm * head_gain)
        .astype(jnp.bfloat16)
        .reshape(row_count, local_heads * value_size)
    )
    mixed = jnp.dot(
        lax.all_gather(head_out, "tp", axis=1, tiled=True),
        out_weight,
        preferred_element_type=jnp.float32,
    )
    return mixed.astype(jnp.bfloat16)


def expert_block(
    routed_in,
    routed_gain,
    expert_ids,
    group_logits,
    inner_logits,
    gate_weight,
    up_weight,
    down_weight,
):
    token_count = routed_in.shape[0]
    chosen = expert_ids.shape[1]
    ep_size = lax.axis_size(EP)
    capacity = 2 * chosen * token_count // ep_size
    source = routed_in.astype(jnp.float32)
    normed = (
        source
        * lax.rsqrt(jnp.mean(source * source, axis=-1, keepdims=True) + EPSILON)
        * routed_gain
    ).astype(jnp.bfloat16)
    flat_ids = expert_ids.reshape(-1)
    picked = (flat_ids[:, None] == jnp.arange(ep_size, dtype=jnp.int32)[None, :]).astype(jnp.int32)
    slot_index = jnp.sum(jnp.cumsum(picked, axis=0) * picked, axis=1) - 1
    place_index = flat_ids * capacity + slot_index
    owner_row = jnp.arange(token_count * chosen, dtype=jnp.int32) // chosen
    slot_rows = jnp.zeros((ep_size * capacity,), jnp.int32).at[place_index].set(owner_row)
    outgoing = normed[slot_rows].reshape(ep_size, capacity, normed.shape[1])
    gate_local = gate_weight[0]
    up_local = up_weight[0]
    down_local = down_weight[0]
    columns = outgoing.shape[2] // lax.axis_size("tp")
    own_columns = lax.dynamic_slice_in_dim(outgoing, lax.axis_index("tp") * columns, columns, 2)
    arrived = lax.all_to_all(own_columns, EP, split_axis=0, concat_axis=0, tiled=True)
    experts_arrived = lax.all_gather(arrived, "tp", axis=2, tiled=True)
    stacked = experts_arrived.reshape(-1, experts_arrived.shape[2])
    gate_act = jnp.dot(stacked, gate_local, preferred_element_type=jnp.float32)
    up_act = jnp.dot(stacked, up_local, preferred_element_type=jnp.float32)
    hidden = (jax.nn.silu(gate_act) * up_act).astype(jnp.bfloat16)
    partial_value = jnp.dot(hidden, down_local, preferred_element_type=jnp.float32)
    partial_value = partial_value.reshape(
        experts_arrived.shape[0], experts_arrived.shape[1], partial_value.shape[1]
    )
    answered = lax.psum_scatter(
        partial_value.astype(jnp.bfloat16), "tp", scatter_dimension=2, tiled=True
    )
    returned = lax.all_to_all(answered, EP, split_axis=0, concat_axis=0, tiled=True)
    pair_out = returned.reshape(ep_size * capacity, returned.shape[2])[place_index]
    pair_out = pair_out.reshape(token_count, chosen, returned.shape[2])
    group_prob = jax.nn.softmax(group_logits, axis=-1)
    member = (
        expert_ids[..., None] // GROUP_SIZE == jnp.arange(group_logits.shape[1], dtype=jnp.int32)
    ).astype(jnp.float32)
    group_pick = jnp.sum(group_prob[:, None, :] * member, axis=-1)
    route_weight = group_pick * jax.nn.softmax(inner_logits, axis=-1)
    return jnp.sum(route_weight[..., None] * pair_out.astype(jnp.float32), axis=1).astype(
        jnp.bfloat16
    )


def local(
    queries,
    key_rows,
    values,
    second_scale,
    head_gain,
    out_weight,
    routed_in,
    routed_gain,
    expert_ids,
    group_logits,
    inner_logits,
    gate_weight,
    up_weight,
    down_weight,
):
    mixer_out = token_mixer(queries, key_rows, values, second_scale, head_gain, out_weight)
    routed_out = expert_block(
        routed_in,
        routed_gain,
        expert_ids,
        group_logits,
        inner_logits,
        gate_weight,
        up_weight,
        down_weight,
    )
    return (mixer_out, routed_out)


def solution(mesh):
    finer = Mesh(mesh.devices.reshape(8, 4, mesh.shape["tp"]), ("ep_0", "ep_1", "tp"))
    placed = (
        P(EP, "tp"),
        P(EP, "tp"),
        P(EP, "tp"),
        P("tp"),
        P(),
        P(None, "tp"),
        P(EP, None),
        P(),
        P(EP, None),
        P(EP, None),
        P(EP, None),
        P(EP, None, "tp"),
        P(EP, None, "tp"),
        P(EP, "tp", None),
    )
    return jax.shard_map(
        local, mesh=finer, in_specs=placed, out_specs=(P(EP, "tp"), P(EP, "tp")), check_vma=False
    )
```

profile of v0, /device:TPU:1, one launch (start us, length us, event | category | flops | bytes accessed | tf_op | source)
XLA Modules:
  0.0 325.3 jit_solution(6230517476498490236)
XLA Ops:
  7.2 0.9 copy.52
  8.4 0.7 and_select_fusion
  9.1 1.2 reduce-window.6
  11.0 2.4 scatter_custom_fusion
  13.5 1.5 fusion.21
  15.0 1.5 fusion.23
  16.6 6.0 %gather_fusion = bf16[1024,2048]{1,0:T(8,128)(2,1)} fusion(bf16[256,2048]{1,0:T(8,128)(2,1)S(1)} %fusion.23, s32[1024]{0:T(1024)S(1)} %fusion.38), kind=kCustom, calls=%fused_computation | custom fusion | bytes 8392704 | tf_op jit(solution)/shard_map/gather | solution.py:123
  22.6 1.0 constant_dynamic-slice_fusion
  23.5 24.9 %all_to_all.10 = bf16[32,32,128]{2,1,0:T(8,128)(2,1)} all-to-all(bf16[32,32,128]{2,1,0:T(8,128)(2,1)S(1)} %constant_dynamic-slice_fusion), channel_id=1, replica_groups=mesh['ep_0'=8,'ep_1'=4,'tp'=16] {'ep_0','ep_1'}, dimensions={0} | all-to-all | bytes 524288 | tf_op jit(solution)/shard_map/all_to_all | solution.py:129
  48.6 10.7 %all_gather.18 = bf16[1024,128]{1,0:T(8,128)(2,1)} all-gather(bf16[256,128]{1,0:T(8,128)(2,1)S(1)} %copy-done.3), channel_id=1, replica_groups=mesh['ep_0'=8,'ep_1'=4,'tp'=16] {'ep_1'}, dimensions={0}, use_global_device_ids=true | all-gather | bytes 327680 | tf_op jit(solution)/shard_map/all_gather | solution.py:17
  59.4 11.1 %all_gather.20 = bf16[1024,128]{1,0:T(8,128)(2,1)} all-gather(bf16[256,128]{1,0:T(8,128)(2,1)S(1)} %copy-done.4), channel_id=1, replica_groups=mesh['ep_0'=8,'ep_1'=4,'tp'=16] {'ep_1'}, dimensions={0}, use_global_device_ids=true | all-gather | bytes 327680 | tf_op jit(solution)/shard_map/all_gather | solution.py:17
  70.6 28.3 %all-gather.11.cloned.1.call-done = bf16[32,32,2048]{2,1,0:T(8,128)(2,1)} async-done(((bf16[32,32,128]{2,1,0:T(8,128)(2,1)}), bf16[32,32,2048]{2,1,0:T(8,128)(2,1)}) %all-gather.11.cloned.1.call-update) | async-done | bytes 4194320 | tf_op jit(solution)/shard_map/all_gather | solution.py:130
  98.8 3.6 %fusion.27 = f32[1024,256]{1,0:T(8,128)S(1)} fusion(bf16[1024,2048]{1,0:T(8,128)(2,1)} %bitcast.107, bf16[1,2048,256]{2,1,0:T(8,128)(2,1)S(1)} %copy-done.9), kind=kOutput, calls=%fused_computation.42 | convolution fusion | flops 1073741824 | bytes 6291456 | tf_op jit(solution)/shard_map/dot_general | solution.py:132
  102.4 1.3 fusion.24
  103.7 3.2 convolution_convert_fusion
  106.9 23.0 %copy.58 = bf16[32,32,2048]{1,0,2:T(8,128)(2,1)} copy(bf16[32,32,2048]{2,1,0:T(8,128)(2,1)} %convolution_convert_fusion) | data formatting | bytes 8388608
  130.0 23.3 %reshape.280 = bf16[2048,1024]{1,0:T(8,128)(2,1)} reshape(bf16[2048,32,32]{2,1,0:T(8,128)(2,1)} %bitcast.93) | data formatting | bytes 8388608
  154.9 8.2 %reshape.279 = bf16[16,512,1,2,64]{4,3,1,0,2:T(2,128)(2,1)} reshape(bf16[8192,128]{1,0:T(8,128)(2,1)} %all-gather.5.cloned.1.call-done) | data formatting | bytes 4194304 | tf_op jit(solution)/shard_map/reshape | solution.py:42
  163.1 9.1 %copy.48 = bf16[16,512,1,2,64]{1,4,3,2,0:T(8,128)(2,1)S(1)} copy(bf16[16,512,1,2,64]{4,3,1,0,2:T(2,128)(2,1)} %reshape.279) | data formatting | bytes 4194304
  172.2 10.3 %all-gather.7.cloned.1.call-done = bf16[8192,128]{1,0:T(8,128)(2,1)} async-done(((bf16[1024,128]{1,0:T(8,128)(2,1)}), bf16[8192,128]{1,0:T(8,128)(2,1)}) %all-gather.7.cloned.1.call-update) | async-done | bytes 2097168 | tf_op jit(solution)/shard_map/all_gather | solution.py:17
  182.6 3.9 %copy.49 = bf16[16,512,1,128]{1,3,2,0:T(8,128)(2,1)} copy(bf16[16,512,1,128]{3,1,0,2:T(8,128)(2,1)} %bitcast.98) | data formatting | bytes 4194304
  186.6 24.3 %while.15 = (s32[]{:T(128)}, f32[256,1,2]{0,2,1:T(2,128)S(1)}, f32[256,1,2]{0,2,1:T(2,128)S(1)}, f32[256,1,2,128]{0,3,2,1:T(8,128)S(1)}, s32[16]{0:T(128)S(1)}, ...) while((s32[]{:T(128)}, f32[256,1,2]{0,2,1:T(2,128)S(1)}, ...), condition=%wide.region_5.6_spmd.clone, body=%wide.region_0.5_spmd.clone.sunk | while | flops 103287040 | bytes 4563285 | solution.py:79
  186.6 0.6 dynamic_slice.27
  187.8 4.0 %conditional.3 = ((f32[256,1,2]{0,2,1:T(2,128)S(1)}, f32[256,1,2]{0,2,1:T(2,128)S(1)}, f32[256,1,2,128]{0,3,2,1:T(8,128)S(1)})) conditional(s32[]{:T(128)} %convert_element_type.73, (f32[256,1,2]{0,2,1:T(2,128)S(1)}, f32[256,1,2]{0,2,1:T(2,128)S(1)}, f32[256,1,2,128]{0,3,2,1:T(8,128)S(1)}) %tuple.42, (s32[]{:T(128)}, s32[]{:T(128)}, s32[]{:T(128)}, ...), branch_computations={%region_1.1_spmd, %region_2.4_spmd} | conditional | flops 103287040 | bytes 4562002 | solution.py:75
  190.3 1.3 fusion.4
  191.8 0.6 dynamic_slice.27
  193.1 0.6 dynamic_slice.27
  194.4 0.6 dynamic_slice.27
  195.6 0.6 dynamic_slice.27
  196.9 0.6 dynamic_slice.27
  198.2 0.6 dynamic_slice.27
  199.5 0.6 dynamic_slice.27
  200.7 0.6 dynamic_slice.27
  202.0 0.6 dynamic_slice.27
  203.3 0.6 dynamic_slice.27
  204.5 0.6 dynamic_slice.27
  205.8 0.6 dynamic_slice.27
  207.1 0.6 dynamic_slice.27
  208.3 0.6 dynamic_slice.27
  211.0 0.7 fusion.32
  211.9 39.5 %reduce-scatter.4.cloned.1.call-done = bf16[128,1024]{1,0:T(8,128)(2,1)} async-done(((bf16[2048,1024]{1,0:T(8,128)(2,1)}), bf16[128,1024]{1,0:T(8,128)(2,1)}) %reduce-scatter.4.cloned.1.call-update) | async-done | bytes 262160
  251.4 1.8 reshape.281
  253.3 1.8 copy.59
  255.1 25.9 %all-to-all-start.1 = ((bf16[32,32,128]{2,1,0:T(8,128)(2,1)}), bf16[32,32,128]{2,1,0:T(8,128)(2,1)S(1)}, u32[]{:S(2)}, u32[]{:S(2)}) async-start(bf16[32,32,128]{2,1,0:T(8,128)(2,1)} %copy.59), calls=%async_computation.1 | async-start | bytes 524288 | tf_op jit(solution)/shard_map/all_to_all | solution.py:142
  281.1 32.9 %all-gather.9.cloned.1.call-done = bf16[256,2048]{0,1:T(8,128)(2,1)} async-done(((bf16[256,128]{0,1:T(8,128)(2,1)}), bf16[256,2048]{0,1:T(8,128)(2,1)}) %all-gather.9.cloned.1.call-update) | async-done | bytes 1048592 | tf_op jit(solution)/shard_map/all_gather | solution.py:90
  314.0 2.3 convolution_convert_fusion.1
  316.4 1.3 gather_fusion.1
  317.7 1.1 fusion.29
  (105 shorter events, 4.2 us)
Async XLA Ops:
  7.2 96.6 %copy-start = (bf16[1,256,2048]{2,1,0:T(8,128)(2,1)S(1)}, bf16[1,256,2048]{2,1,0:T(8,128)(2,1)}, u32[]{:S(2)}) copy-start(bf16[1,256,2048]{2,1,0:T(8,128)(2,1)} %param.31) | copy-start | bytes 3145732
  7.2 91.6 %all-gather.11.cloned.1.call-start = ((), (), s32[]{:S(2)}) async-start(), calls=%async_computation.6 | async-start | bytes 4456448 | tf_op jit(solution)/shard_map/all_gather | solution.py:130
  16.5 32.0 %copy-start.3 = (bf16[256,128]{1,0:T(8,128)(2,1)S(1)}, bf16[256,128]{1,0:T(8,128)(2,1)}, u32[]{:S(2)}) copy-start(bf16[256,128]{1,0:T(8,128)(2,1)} %param.19) | copy-start | bytes 196612
  16.5 42.8 %copy-start.4 = (bf16[256,128]{1,0:T(8,128)(2,1)S(1)}, bf16[256,128]{1,0:T(8,128)(2,1)}, u32[]{:S(2)}) copy-start(bf16[256,128]{1,0:T(8,128)(2,1)} %param.20) | copy-start | bytes 196612
  16.5 82.3 %copy-start.9 = (bf16[1,2048,256]{2,1,0:T(8,128)(2,1)S(1)}, bf16[1,2048,256]{2,1,0:T(8,128)(2,1)}, u32[]{:S(2)}) copy-start(bf16[1,2048,256]{2,1,0:T(8,128)(2,1)} %param.29) | copy-start | bytes 3145732
  48.5 106.4 %all-gather.5.cloned.1.call-start = ((), (), s32[]{:S(2)}) async-start(), calls=%async_computation.3 | async-start | bytes 2359296 | tf_op jit(solution)/shard_map/all_gather | solution.py:17
  59.3 43.2 %copy-start.10 = (bf16[1,2048,256]{2,1,0:T(8,128)(2,1)S(1)}, bf16[1,2048,256]{2,1,0:T(8,128)(2,1)}, u32[]{:S(2)}) copy-start(bf16[1,2048,256]{2,1,0:T(8,128)(2,1)} %param.30) | copy-start | bytes 3145732
  59.3 123.3 %all-gather.7.cloned.1.call-start = ((), (), s32[]{:S(2)}) async-start(), calls=%async_computation.4 | async-start | bytes 2359296 | tf_op jit(solution)/shard_map/all_gather | solution.py:17
  70.5 180.9 %reduce-scatter.4.cloned.1.call-start = ((), (), s32[]{:S(2)}) async-start(), calls=%async_computation.7 | async-start | bytes 4456448
  98.8 3.6 %copy-start.8 = (bf16[32,32,2048]{2,1,0:T(8,128)(2,1)S(1)}, bf16[32,32,2048]{2,1,0:T(8,128)(2,1)}, u32[]{:S(2)}) copy-start(bf16[32,32,2048]{2,1,0:T(8,128)(2,1)} %all-gather.11.cloned.1.call-done) | copy-start | bytes 12582916
  153.3 0.8 copy-start.5
  153.3 160.7 %all-gather.9.cloned.1.call-start = ((), (), s32[]{:S(2)}) async-start(), calls=%async_computation.5 | async-start | bytes 1114112 | tf_op jit(solution)/shard_map/all_gather | solution.py:90
  186.5 24.4 %copy-start.7 = (f32[128]{0:T(128)S(1)}, f32[128]{0:T(128)}, u32[]{:S(2)}) copy-start(f32[128]{0:T(128)} %param.22) | copy-start | bytes 1540
  186.6 25.2 %copy-start.2 = (f32[256,8]{0,1:T(8,128)S(1)}, f32[256,8]{0,1:T(8,128)}, u32[]{:S(2)}) copy-start(f32[256,8]{0,1:T(8,128)} %param.27) | copy-start | bytes 24580
  186.6 25.2 %copy-start.6 = (f32[256,2]{0,1:T(2,128)S(1)}, f32[256,2]{0,1:T(2,128)}, u32[]{:S(2)}) copy-start(f32[256,2]{0,1:T(2,128)} %param.28) | copy-start | bytes 6148
  210.9 103.1 %copy-start.1 = (bf16[2048,128]{1,0:T(8,128)(2,1)S(1)}, bf16[2048,128]{1,0:T(8,128)(2,1)}, u32[]{:S(2)}) copy-start(bf16[2048,128]{1,0:T(8,128)(2,1)} %param.23) | copy-start | bytes 1572868
  255.1 61.3 %all-to-all-start.1 = ((bf16[32,32,128]{2,1,0:T(8,128)(2,1)}), bf16[32,32,128]{2,1,0:T(8,128)(2,1)S(1)}, u32[]{:S(2)}, u32[]{:S(2)}) async-start(bf16[32,32,128]{2,1,0:T(8,128)(2,1)} %copy.59), calls=%async_computation.1 | async-start | bytes 524288 | tf_op jit(solution)/shard_map/all_to_all | solution.py:142
Sparse Core Ops, SparseCore 0:
  48.6 50.1 all-gather.10
  100.9 37.4 all-gather.4
  140.5 42.0 all-gather.6
  185.3 66.1 reduce-scatter.3
  254.0 59.9 all-gather.8
where the time goes:
time: 328 us; the launch traced here: 325 us
  waiting for transfers between devices  111 us (34%)
  local copies, waits for them, and re-layouts  94.1 us (29%)
  blocking collectives  46.8 us (14%)
  starting transfers between devices  26.3 us (8%)
  between operations  14.8 us (5%)
  loops' own time  12.6 us (4%)
  matrix products  12.1 us (4%)
  other arithmetic  7.48 us (2%)
    unnamed x30, local copies, waits for them, and re-layouts  64.6 us
    unnamed x6, waiting for transfers between devices  39.6 us
    all_gather x1, waiting for transfers between devices, token_mixer(): lax.all_gather(head_out, 'tp', axis=1, tiled=True)  32.9 us
    all_gather x1, waiting for transfers between devices, expert_block(): experts_arrived = lax.all_gather(arrived, 'tp', axis=2, tiled=True)  28.3 us
    all_to_all x1, starting transfers between devices, expert_block(): lax.all_to_all(answered, EP, split_axis=0, concat_axis=0, tiled=True)  25.9 us
    all_to_all x1, blocking collectives, expert_block(): lax.all_to_all(own_columns, EP, split_axis=0, concat_axis=0, tiled=True)  24.9 us
    all_gather x2, blocking collectives, whole_of(): nearer = lax.all_gather(array, axes[-1], axis=dim, tiled=True)  21.8 us
    another operation x1, loops' own time, token_mixer(): lax.scan(update, state_now, jnp.arange(blocks, dtype=jnp.int32))  10.6 us
  transfers between devices with their start and end apart: 6, of which 4 were waited for; matrix products, arithmetic and copies ran while one was open for 29% of the time, Pallas kernels for 0%

commit v1 on v0

--- a/solution.py
+++ b/solution.py
@@ -9,6 +9,11 @@
 EP = ("ep_0", "ep_1")
 EPSILON = 1e-05
 LOWEST = -1e30
+
+
+def tiled_gather(array, axis, dim):
+    copies = jnp.concatenate([array] * lax.axis_size(axis), axis=dim)
+    return lax.all_to_all(copies, axis, dim, dim, tiled=True)
 
 
 def whole_of(array, axes, dim):
@@ -86,11 +91,7 @@
         .astype(jnp.bfloat16)
         .reshape(row_count, local_heads * value_size)
     )
-    mixed = jnp.dot(
-        lax.all_gather(head_out, "tp", axis=1, tiled=True),
-        out_weight,
-        preferred_element_type=jnp.float32,
-    )
+    mixed = jnp.dot(tiled_gather(head_out, "tp", 1), out_weight, preferred_element_type=jnp.float32)
     return mixed.astype(jnp.bfloat16)
 
 

time: 328 us -> 341 us (1.040)
  starting transfers between devices: 26.3 us -> 56.6 us
  waiting for transfers between devices: 111 us -> 91.9 us
    all_gather x1 -> x0, waiting for transfers between devices: 32.9 us -> none  [token_mixer(): lax.all_gather(head_out, 'tp', axis=1, tiled=True)]
    all_to_all x1, starting transfers between devices: 25.9 us -> 45.1 us  [expert_block(): lax.all_to_all(answered, EP, split_axis=0, concat_axis=0, tiled=True)]
    all_to_all x0 -> x1, starting transfers between devices: none -> 11.2 us  [tiled_gather(): return lax.all_to_all(copies, axis, dim, dim, tiled=True)]
    all_to_all x1, waiting for transfers between devices: 0.01 us -> 8.67 us  [expert_block(): lax.all_to_all(answered, EP, split_axis=0, concat_axis=0, tiled=True)]
    unnamed x6 -> x5, waiting for transfers between devices: 39.6 us -> 44.7 us
    unnamed x30 -> x28, local copies, waits for them, and re-layouts: 64.6 us -> 64.8 us
where the time goes in v1:
time: 341 us; the launch traced here: 339 us
  local copies, waits for them, and re-layouts  97 us (28%)
  waiting for transfers between devices  91.9 us (27%)
  starting transfers between devices  56.6 us (17%)
  blocking collectives  46.8 us (14%)
  between operations  14.8 us (4%)
  loops' own time  12.6 us (4%)
  matrix products  12.2 us (4%)
  other arithmetic  6.86 us (2%)
    unnamed x28, local copies, waits for them, and re-layouts  64.8 us
    all_to_all x1, starting transfers between devices, expert_block(): lax.all_to_all(answered, EP, split_axis=0, concat_axis=0, tiled=True)  45.1 us
    unnamed x5, waiting for transfers between devices  44.7 us
    all_gather x1, waiting for transfers between devices, expert_block(): experts_arrived = lax.all_gather(arrived, 'tp', axis=2, tiled=True)  28.1 us
    all_to_all x1, blocking collectives, expert_block(): lax.all_to_all(own_columns, EP, split_axis=0, concat_axis=0, tiled=True)  24.9 us
    all_gather x2, blocking collectives, whole_of(): nearer = lax.all_gather(array, axes[-1], axis=dim, tiled=True)  21.8 us
    all_to_all x1, starting transfers between devices, tiled_gather(): return lax.all_to_all(copies, axis, dim, dim, tiled=True)  11.2 us
    another operation x1, loops' own time, token_mixer(): lax.scan(update, state_now, jnp.arange(blocks, dtype=jnp.int32))  10.6 us
  transfers between devices with their start and end apart: 6, of which 4 were waited for; matrix products, arithmetic and copies ran while one was open for 29% of the time, Pallas kernels for 0%

profile of v1, /device:TPU:1, one launch (start us, length us, event | category | flops | bytes accessed | tf_op | source)
XLA Modules:
  0.0 338.8 jit_solution(11611852328548836392)
XLA Ops:
  7.2 0.9 copy.71
  8.4 0.7 and_select_fusion
  9.1 1.2 reduce-window.6
  11.0 2.4 scatter_custom_fusion
  13.5 1.5 fusion.21
  15.0 1.5 fusion.23
  16.6 6.0 %gather_fusion = bf16[1024,2048]{1,0:T(8,128)(2,1)} fusion(bf16[256,2048]{1,0:T(8,128)(2,1)S(1)} %fusion.23, s32[1024]{0:T(1024)S(1)} %fusion.38), kind=kCustom, calls=%fused_computation | custom fusion | bytes 8392704 | tf_op jit(solution)/shard_map/gather | solution.py:124
  22.6 1.0 constant_dynamic-slice_fusion
  23.5 24.9 %all_to_all.19 = bf16[32,32,128]{2,1,0:T(8,128)(2,1)} all-to-all(bf16[32,32,128]{2,1,0:T(8,128)(2,1)S(1)} %constant_dynamic-slice_fusion), channel_id=1, replica_groups=mesh['ep_0'=8,'ep_1'=4,'tp'=16] {'ep_0','ep_1'}, dimensions={0} | all-to-all | bytes 524288 | tf_op jit(solution)/shard_map/all_to_all | solution.py:130
  48.6 10.7 %all_gather.15 = bf16[1024,128]{1,0:T(8,128)(2,1)} all-gather(bf16[256,128]{1,0:T(8,128)(2,1)S(1)} %copy-done.2), channel_id=1, replica_groups=mesh['ep_0'=8,'ep_1'=4,'tp'=16] {'ep_1'}, dimensions={0}, use_global_device_ids=true | all-gather | bytes 327680 | tf_op jit(solution)/shard_map/all_gather | solution.py:22
  59.4 11.1 %all_gather.17 = bf16[1024,128]{1,0:T(8,128)(2,1)} all-gather(bf16[256,128]{1,0:T(8,128)(2,1)S(1)} %copy-done.3), channel_id=1, replica_groups=mesh['ep_0'=8,'ep_1'=4,'tp'=16] {'ep_1'}, dimensions={0}, use_global_device_ids=true | all-gather | bytes 327680 | tf_op jit(solution)/shard_map/all_gather | solution.py:22
  70.7 28.1 %all-gather.8.cloned.1.call-done = bf16[32,32,2048]{2,1,0:T(8,128)(2,1)} async-done(((bf16[32,32,128]{2,1,0:T(8,128)(2,1)}), bf16[32,32,2048]{2,1,0:T(8,128)(2,1)}) %all-gather.8.cloned.1.call-update) | async-done | bytes 4194320 | tf_op jit(solution)/shard_map/all_gather | solution.py:131
  98.8 3.6 %fusion.27 = f32[1024,256]{1,0:T(8,128)S(1)} fusion(bf16[1024,2048]{1,0:T(8,128)(2,1)} %bitcast.109, bf16[1,2048,256]{2,1,0:T(8,128)(2,1)S(1)} %copy-done.8), kind=kOutput, calls=%fused_computation.42 | convolution fusion | flops 1073741824 | bytes 6291456 | tf_op jit(solution)/shard_map/dot_general | solution.py:133
  102.4 1.3 fusion.24
  103.7 3.2 convolution_convert_fusion
  106.9 23.0 %copy.77 = bf16[32,32,2048]{1,0,2:T(8,128)(2,1)} copy(bf16[32,32,2048]{2,1,0:T(8,128)(2,1)} %convolution_convert_fusion) | data formatting | bytes 8388608
  130.0 23.3 %reshape.457 = bf16[2048,1024]{1,0:T(8,128)(2,1)} reshape(bf16[2048,32,32]{2,1,0:T(8,128)(2,1)} %bitcast.94) | data formatting | bytes 8388608
  153.3 0.8 copy-done.4
  154.9 8.2 %reshape.456 = bf16[16,512,1,2,64]{4,3,1,0,2:T(2,128)(2,1)} reshape(bf16[8192,128]{1,0:T(8,128)(2,1)} %all-gather.4.cloned.1.call-done) | data formatting | bytes 4194304 | tf_op jit(solution)/shard_map/reshape | solution.py:47
  163.1 9.1 %copy.65 = bf16[16,512,1,2,64]{1,4,3,2,0:T(8,128)(2,1)S(1)} copy(bf16[16,512,1,2,64]{4,3,1,0,2:T(2,128)(2,1)} %reshape.456) | data formatting | bytes 4194304
  172.2 10.4 %all-gather.6.cloned.1.call-done = bf16[8192,128]{1,0:T(8,128)(2,1)} async-done(((bf16[1024,128]{1,0:T(8,128)(2,1)}), bf16[8192,128]{1,0:T(8,128)(2,1)}) %all-gather.6.cloned.1.call-update) | async-done | bytes 2097168 | tf_op jit(solution)/shard_map/all_gather | solution.py:22
  182.7 3.9 %copy.66 = bf16[16,512,1,128]{1,3,2,0:T(8,128)(2,1)} copy(bf16[16,512,1,128]{3,1,0,2:T(8,128)(2,1)} %bitcast.100) | data formatting | bytes 4194304
  186.7 24.3 %while.15 = (s32[]{:T(128)}, f32[256,1,2]{0,2,1:T(2,128)S(1)}, f32[256,1,2]{0,2,1:T(2,128)S(1)}, f32[256,1,2,128]{0,3,2,1:T(8,128)S(1)}, s32[16]{0:T(128)S(1)}, ...) while((s32[]{:T(128)}, f32[256,1,2]{0,2,1:T(2,128)S(1)}, ...), condition=%wide.region_5.6_spmd.clone, body=%wide.region_0.5_spmd.clone.sunk | while | flops 103287040 | bytes 4563285 | solution.py:84
  187.9 4.0 %conditional.3 = ((f32[256,1,2]{0,2,1:T(2,128)S(1)}, f32[256,1,2]{0,2,1:T(2,128)S(1)}, f32[256,1,2,128]{0,3,2,1:T(8,128)S(1)})) conditional(s32[]{:T(128)} %convert_element_type.92, (f32[256,1,2]{0,2,1:T(2,128)S(1)}, f32[256,1,2]{0,2,1:T(2,128)S(1)}, f32[256,1,2,128]{0,3,2,1:T(8,128)S(1)}) %tuple.43, (s32[]{:T(128)}, s32[]{:T(128)}, s32[]{:T(128)}, ...), branch_computations={%region_1.1_spmd, %region_2.4_spmd} | conditional | flops 103287040 | bytes 4562002 | solution.py:80
  190.3 1.3 fusion.4
  191.9 0.6 dynamic_slice.27
  193.2 0.6 dynamic_slice.27
  194.5 0.6 dynamic_slice.27
  195.7 0.6 dynamic_slice.27
  197.0 0.6 dynamic_slice.27
  198.3 0.6 dynamic_slice.27
  199.5 0.6 dynamic_slice.27
  200.8 0.6 dynamic_slice.27
  202.1 0.6 dynamic_slice.27
  203.3 0.6 dynamic_slice.27
  205.9 0.6 dynamic_slice.27
  207.1 0.6 dynamic_slice.27
  211.3 1.2 concatenate.4
  212.5 11.2 %all-to-all-start = ((bf16[256,16,128]{2,0,1:T(8,128)(2,1)}), bf16[256,16,128]{2,0,1:T(8,128)(2,1)S(1)}, u32[]{:S(2)}, u32[]{:S(2)}) async-start(bf16[256,16,128]{2,0,1:T(8,128)(2,1)} %concatenate.4), calls=%async_computation | async-start | bytes 2097152 | tf_op jit(solution)/shard_map/all_to_all | solution.py:16
  223.8 44.7 %reduce-scatter.4.cloned.1.call-done = bf16[128,1024]{1,0:T(8,128)(2,1)} async-done(((bf16[2048,1024]{1,0:T(8,128)(2,1)}), bf16[128,1024]{1,0:T(8,128)(2,1)}) %reduce-scatter.4.cloned.1.call-update) | async-done | bytes 262160
  268.5 1.8 reshape.458
  270.3 1.8 copy.78
  272.1 45.1 %all-to-all-start.2 = ((bf16[32,32,128]{2,1,0:T(8,128)(2,1)}), bf16[32,32,128]{2,1,0:T(8,128)(2,1)S(1)}, u32[]{:S(2)}, u32[]{:S(2)}) async-start(bf16[32,32,128]{2,1,0:T(8,128)(2,1)} %copy.78), calls=%async_computation.2 | async-start | bytes 524288 | tf_op jit(solution)/shard_map/all_to_all | solution.py:143
  317.4 1.3 copy.68
  318.7 2.5 convolution_convert_fusion.1
  321.2 8.7 %all-to-all-done.2 = bf16[32,32,128]{2,1,0:T(8,128)(2,1)S(1)} async-done(((bf16[32,32,128]{2,1,0:T(8,128)(2,1)}), bf16[32,32,128]{2,1,0:T(8,128)(2,1)S(1)}, u32[]{:S(2)}, u32[]{:S(2)}) %all-to-all-start.2) | async-done | bytes 262176 | tf_op jit(solution)/shard_map/all_to_all | solution.py:143
  329.9 1.3 gather_fusion.1
  331.2 1.1 fusion.29
  (105 shorter events, 5.5 us)
Async XLA Ops:
  7.2 96.6 %copy-start = (bf16[1,256,2048]{2,1,0:T(8,128)(2,1)S(1)}, bf16[1,256,2048]{2,1,0:T(8,128)(2,1)}, u32[]{:S(2)}) copy-start(bf16[1,256,2048]{2,1,0:T(8,128)(2,1)} %param.31) | copy-start | bytes 3145732
  7.2 91.6 %all-gather.8.cloned.1.call-start = ((), (), s32[]{:S(2)}) async-start(), calls=%async_computation.6 | async-start | bytes 4456448 | tf_op jit(solution)/shard_map/all_gather | solution.py:131
  16.5 32.0 %copy-start.2 = (bf16[256,128]{1,0:T(8,128)(2,1)S(1)}, bf16[256,128]{1,0:T(8,128)(2,1)}, u32[]{:S(2)}) copy-start(bf16[256,128]{1,0:T(8,128)(2,1)} %param.19) | copy-start | bytes 196612
  16.5 42.8 %copy-start.3 = (bf16[256,128]{1,0:T(8,128)(2,1)S(1)}, bf16[256,128]{1,0:T(8,128)(2,1)}, u32[]{:S(2)}) copy-start(bf16[256,128]{1,0:T(8,128)(2,1)} %param.20) | copy-start | bytes 196612
  16.5 82.3 %copy-start.8 = (bf16[1,2048,256]{2,1,0:T(8,128)(2,1)S(1)}, bf16[1,2048,256]{2,1,0:T(8,128)(2,1)}, u32[]{:S(2)}) copy-start(bf16[1,2048,256]{2,1,0:T(8,128)(2,1)} %param.29) | copy-start | bytes 3145732
  48.5 106.4 %all-gather.4.cloned.1.call-start = ((), (), s32[]{:S(2)}) async-start(), calls=%async_computation.4 | async-start | bytes 2359296 | tf_op jit(solution)/shard_map/all_gather | solution.py:22
  59.3 43.2 %copy-start.9 = (bf16[1,2048,256]{2,1,0:T(8,128)(2,1)S(1)}, bf16[1,2048,256]{2,1,0:T(8,128)(2,1)}, u32[]{:S(2)}) copy-start(bf16[1,2048,256]{2,1,0:T(8,128)(2,1)} %param.30) | copy-start | bytes 3145732
  59.3 123.4 %all-gather.6.cloned.1.call-start = ((), (), s32[]{:S(2)}) async-start(), calls=%async_computation.5 | async-start | bytes 2359296 | tf_op jit(solution)/shard_map/all_gather | solution.py:22
  70.5 198.0 %reduce-scatter.4.cloned.1.call-start = ((), (), s32[]{:S(2)}) async-start(), calls=%async_computation.7 | async-start | bytes 4456448
  98.8 3.6 %copy-start.7 = (bf16[32,32,2048]{2,1,0:T(8,128)(2,1)S(1)}, bf16[32,32,2048]{2,1,0:T(8,128)(2,1)}, u32[]{:S(2)}) copy-start(bf16[32,32,2048]{2,1,0:T(8,128)(2,1)} %all-gather.8.cloned.1.call-done) | copy-start | bytes 12582916
  153.3 0.8 copy-start.4
  186.7 24.4 %copy-start.6 = (f32[128]{0:T(128)S(1)}, f32[128]{0:T(128)}, u32[]{:S(2)}) copy-start(f32[128]{0:T(128)} %param.22) | copy-start | bytes 1540
  210.9 12.7 %copy-start.1 = (f32[256,8]{0,1:T(8,128)S(1)}, f32[256,8]{0,1:T(8,128)}, u32[]{:S(2)}) copy-start(f32[256,8]{0,1:T(8,128)} %param.27) | copy-start | bytes 24580
  210.9 12.7 %copy-start.5 = (f32[256,2]{0,1:T(2,128)S(1)}, f32[256,2]{0,1:T(2,128)}, u32[]{:S(2)}) copy-start(f32[256,2]{0,1:T(2,128)} %param.28) | copy-start | bytes 6148
  212.5 59.6 %all-to-all-start = ((bf16[256,16,128]{2,0,1:T(8,128)(2,1)}), bf16[256,16,128]{2,0,1:T(8,128)(2,1)S(1)}, u32[]{:S(2)}, u32[]{:S(2)}) async-start(bf16[256,16,128]{2,0,1:T(8,128)(2,1)} %concatenate.4), calls=%async_computation | async-start | bytes 2097152 | tf_op jit(solution)/shard_map/all_to_all | solution.py:16
  272.1 57.8 %all-to-all-start.2 = ((bf16[32,32,128]{2,1,0:T(8,128)(2,1)}), bf16[32,32,128]{2,1,0:T(8,128)(2,1)S(1)}, u32[]{:S(2)}, u32[]{:S(2)}) async-start(bf16[32,32,128]{2,1,0:T(8,128)(2,1)} %copy.78), calls=%async_computation.2 | async-start | bytes 524288 | tf_op jit(solution)/shard_map/all_to_all | solution.py:143
Sparse Core Ops, SparseCore 0:
  48.6 50.1 all-gather.7
  100.9 37.2 all-gather.3
  140.3 42.3 all-gather.5
  185.4 83.0 reduce-scatter.3
